TPU v7x, 32 devices: a whole 2x2x4 slice. The times are simulated.
32 devices in a mesh: ep: 8 (over z, x), tp: 4 (over y, core).
Axes of the slice: x: 2, y: 2, z: 4, core: 2. Of those that a mesh axis runs over, the one named last changes fastest.
Arguments:
- queries: bfloat16 [2048, 1536], P('ep', 'tp'), may hold values from -600 to 600
- compressed_key_value: bfloat16 [2048, 512], P('ep'), may hold values from -6 to 6
- rope_key: bfloat16 [2048, 32], P('ep'), may hold values from -6 to 6
- latent_norm_gain: float32 [512], replicated, may hold values from 0.1 to 1.9
- latent_to_key_value: bfloat16 [512, 2048], P(None, 'tp'), may hold values from -0.25 to 0.25
- out_proj: bfloat16 [1024, 2048], P(None, 'tp'), may hold values from -1.5 to 1.5
- moe_input: bfloat16 [2048, 2048], P('ep'), may hold values from -6 to 6
- moe_gain: float32 [2048], replicated, may hold values from 0.1 to 1.9
- routes: int32 [2048, 2], P('ep'), may hold values from 0 to 7, all different within a row; in each aligned block of 256 rows (0 to 255, 256 to 511, ...) at most 96 rows name the same one
- route_weight: float32 [2048, 2], P('ep'), may hold values from 0.2 to 1
- gate_weight: bfloat16 [8, 2048, 4096], P('ep', None, 'tp'), may hold values from -0.125 to 0.125
- up_weight: bfloat16 [8, 2048, 4096], P('ep', None, 'tp'), may hold values from -0.125 to 0.125
- down_weight: bfloat16 [8, 4096, 2048], P('ep', 'tp'), may hold values from -0.09375 to 0.09375
Outputs:
- attention_out: bfloat16 [2048, 2048], P('ep', 'tp')
- expert_out: bfloat16 [2048, 2048], P('ep', 'tp')
Inputs may be any that keep to these rules, and one draw needn't show every extreme that they name: `routes`: each row names 2 different experts. In the rows of one device (aligned blocks of 256 rows) no expert is named by more than 96 rows, and in some blocks one expert is named by exactly 96 rows.
All inputs are finite; a program needn't handle non-finite values.
Results may differ from a plain program's by a relative error of at most 0.019.
The roundings to bfloat16 on the way count: a program that leaves them out, or rounds other values in their place, can miss the bound.
Values may be sent and summed in bfloat16 or wider, within the bound.
A program may use at most 128 MiB of HBM per device.

v0:
```python
import math

import jax
import jax.numpy as jnp
from jax import lax
from jax.sharding import PartitionSpec as P

PLAIN_HEAD_DIM = 64
ROPE = 32
VALUE_HEAD_DIM = 64


EPSILON = 1e-06
ROPE_BASE_VALUE = 10000.0


def rms_scale(values, gain_vector):
    floats = values.astype(jnp.float32)
    return (
        floats
        * lax.rsqrt(jnp.mean(floats * floats, axis=-1, keepdims=True) + EPSILON)
        * gain_vector
    )


def rotary(values, positions):
    full_width = values.shape[-1]
    half_dim = full_width // 2
    frequency = ROPE_BASE_VALUE ** (-jnp.arange(half_dim, dtype=jnp.float32) * 2.0 / full_width)
    angles = positions[..., None] * frequency
    cosine = jnp.cos(angles)
    sine_part = jnp.sin(angles)
    first_half = values[..., :half_dim]
    second_half = values[..., half_dim:]
    return jnp.concatenate(
        [
            first_half * cosine - second_half * sine_part,
            second_half * cosine + first_half * sine_part,
        ],
        axis=-1,
    )


def slot_table(block_routes, capacity, experts):
    flat_routes = block_routes.reshape(-1)
    onehot_table = (flat_routes[:, None] == jnp.arange(experts, dtype=jnp.int32)[None, :]).astype(
        jnp.int32
    )
    earlier = jnp.cumsum(onehot_table, axis=0) - onehot_table
    slot_index = jnp.sum(earlier * onehot_table, axis=1)
    destination = flat_routes * capacity + slot_index
    token_count = block_routes.shape[0]
    source_rows = jnp.arange(flat_routes.shape[0], dtype=jnp.int32) // block_routes.shape[1]
    source_table = (
        jnp.full((experts * capacity,), token_count, jnp.int32).at[destination].set(source_rows)
    )
    return (destination, source_table)


def local(
    queries,
    compressed_key_value,
    rope_key,
    latent_norm_gain,
    latent_to_key_value,
    out_proj,
    moe_input,
    moe_gain,
    routes,
    route_weight,
    gate_weight,
    up_weight,
    down_weight,
):
    row_count = queries.shape[0]
    head_count = latent_to_key_value.shape[1] // (PLAIN_HEAD_DIM + VALUE_HEAD_DIM)
    offset = lax.axis_index("ep") * row_count
    positions = (offset + jnp.arange(row_count, dtype=jnp.int32)).astype(jnp.float32)
    query_heads = queries.reshape(row_count, head_count, PLAIN_HEAD_DIM + ROPE)
    query_nope = query_heads[..., :PLAIN_HEAD_DIM]
    query_rope = rotary(
        query_heads[..., PLAIN_HEAD_DIM:].astype(jnp.float32), positions[:, None]
    ).astype(jnp.bfloat16)
    latent_normed = rms_scale(compressed_key_value, latent_norm_gain).astype(jnp.bfloat16)
    key_rope = rotary(rope_key.astype(jnp.float32), positions).astype(jnp.bfloat16)
    score_scale = (PLAIN_HEAD_DIM + ROPE) ** (-0.5)

    def attend_block(state_now, key_value, block_rope):
        run_max, run_total, run_values = state_now
        key_nope = key_value[..., :PLAIN_HEAD_DIM]
        block_values = key_value[..., PLAIN_HEAD_DIM:]
        scores = (
            jnp.einsum("qhd,khd->qhk", query_nope, key_nope, preferred_element_type=jnp.float32)
            + jnp.einsum("qhr,kr->qhk", query_rope, block_rope, preferred_element_type=jnp.float32)
        ) * score_scale
        new_max = jnp.maximum(run_max, jnp.max(scores, axis=-1))
        shrink = jnp.exp(run_max - new_max)
        weights = jnp.exp(scores - new_max[..., None])
        run_total = run_total * shrink + jnp.sum(weights, axis=-1)
        run_values = run_values * shrink[..., None] + jnp.einsum(
            "qhk,khd->qhd",
            weights.astype(jnp.bfloat16),
            block_values,
            preferred_element_type=jnp.float32,
        )
        return (new_max, run_total, run_values)

    initial = (
        jnp.full((row_count, head_count), -jnp.inf, jnp.float32),
        jnp.zeros((row_count, head_count), jnp.float32),
        jnp.zeros((row_count, head_count, VALUE_HEAD_DIM), jnp.float32),
    )

    def expand_latent(block_main):
        own_heads = jnp.dot(
            block_main, latent_to_key_value, preferred_element_type=jnp.float32
        ).astype(jnp.bfloat16)
        return own_heads.reshape(block_main.shape[0], head_count, PLAIN_HEAD_DIM + VALUE_HEAD_DIM)

    piece_main = lax.all_gather(latent_normed, "ep", axis=0, tiled=True)
    piece_rope = lax.all_gather(key_rope, "ep", axis=0, tiled=True)
    piece_rows = piece_main.shape[0]
    group_rows = math.gcd(piece_rows, 2048)
    block_count = piece_rows // group_rows
    main_blocks = piece_main.reshape(block_count, group_rows, piece_main.shape[1])
    rope_blocks = piece_rope.reshape(block_count, group_rows, piece_rope.shape[1])

    def step_block(state_inner, block_data):
        block_main, block_rope = block_data
        return (attend_block(state_inner, expand_latent(block_main), block_rope), None)

    state_out, unused = lax.scan(step_block, initial, (main_blocks, rope_blocks))
    run_max, run_total, run_values = state_out
    attended = (
        (run_values / run_total[..., None])
        .astype(jnp.bfloat16)
        .reshape(row_count, head_count * VALUE_HEAD_DIM)
    )
    projected = jnp.dot(
        lax.all_gather(attended, "tp", axis=1, tiled=True),
        out_proj,
        preferred_element_type=jnp.float32,
    )
    attention_out = projected.astype(jnp.bfloat16)
    moe_rows = moe_input.shape[0]
    model_width = moe_input.shape[1]
    expert_local = gate_weight.shape[0]
    ep_count = lax.axis_size("ep")
    tp_count = lax.axis_size("tp")
    expert_total = ep_count * expert_local
    capacity = 3 * moe_rows // ep_count
    normed = rms_scale(moe_input, moe_gain).astype(jnp.bfloat16)
    destination, source_table = slot_table(routes, capacity, expert_total)
    padded = jnp.concatenate([normed, jnp.zeros((1, model_width), jnp.bfloat16)], axis=0)
    outgoing = padded[source_table].reshape(ep_count, expert_local, capacity, model_width)
    column_width = model_width // tp_count
    own_columns = lax.dynamic_slice_in_dim(
        outgoing, lax.axis_index("tp") * column_width, column_width, 3
    )
    arrived_whole = lax.all_gather(
        lax.all_to_all(own_columns, "ep", split_axis=0, concat_axis=0, tiled=True),
        "tp",
        axis=3,
        tiled=True,
    )
    gate_value = jnp.einsum(
        "sexd,edf->sexf", arrived_whole, gate_weight, preferred_element_type=jnp.float32
    )
    up_value = jnp.einsum(
        "sexd,edf->sexf", arrived_whole, up_weight, preferred_element_type=jnp.float32
    )
    hidden = (jax.nn.silu(gate_value) * up_value).astype(jnp.bfloat16)
    partial_out = jnp.einsum(
        "sexf,efd->sexd", hidden, down_weight, preferred_element_type=jnp.float32
    )
    summed = lax.psum_scatter(
        partial_out.astype(jnp.bfloat16), "tp", scatter_dimension=3, tiled=True
    )
    returned = lax.all_to_all(summed, "ep", split_axis=0, concat_axis=0, tiled=True)
    flat_back = returned.reshape(expert_total * capacity, returned.shape[3])
    picked = (
        flat_back[destination]
        .astype(jnp.float32)
        .reshape(moe_rows, routes.shape[1], returned.shape[3])
    )
    expert_out = jnp.sum(picked * route_weight[..., None], axis=1).astype(jnp.bfloat16)
    return (attention_out, expert_out)


def solution(mesh):
    return jax.shard_map(
        local,
        mesh=mesh,
        in_specs=(
            P("ep", "tp"),
            P("ep", None),
            P("ep", None),
            P(),
            P(None, "tp"),
            P(None, "tp"),
            P("ep", None),
            P(),
            P("ep", None),
            P("ep", None),
            P("ep", None, "tp"),
            P("ep", None, "tp"),
            P("ep", "tp", None),
        ),
        out_specs=(P("ep", "tp"), P("ep", "tp")),
        check_vma=False,
    )
```

profile of v0, /device:TPU:0, one launch (start us, length us, event | category | flops | bytes accessed | tf_op | source)
XLA Modules:
  0.0 206.0 jit_solution(7960402563540832148)
XLA Ops:
  7.2 0.0 copy-start
  7.2 0.0 all-gather.5.cloned.1.call-start
  7.2 0.9 copy.30
  8.1 0.1 eq.29
  8.3 0.1 eq.25
  8.4 0.7 broadcast_multiply_fusion
  9.1 1.1 reduce-window.6
  10.3 0.2 slice_reduce_fusion
  10.5 0.1 copy.29
  10.7 0.1 mul.202
  10.8 0.1 fusion.64
  10.9 2.4 %scatter_custom_fusion = s32[768]{0:T(1024)S(1)} fusion(s32[512]{0:T(512)S(1)} %bitcast.124, s32[512]{0:T(512)S(1)} %add_select_fusion, s32[]{:T(128)} %constant.45.clone.1), kind=kCustom, calls=%fused_computation.79 | custom fusion | bytes 3076 | tf_op jit(solution)/shard_map/scatter | solution.py:55
  13.4 1.5 fusion.24
  14.9 1.5 fusion.26
  16.5 0.1 concatenate.13
  16.5 4.3 %gather_fusion = bf16[768,2048]{1,0:T(8,128)(2,1)} fusion(bf16[257,2048]{1,0:T(8,128)(2,1)S(1)} %concatenate.13, s32[1024]{0:T(1024)S(1)} %pad_clamp_fusion.1), kind=kCustom, calls=%fused_computation | custom fusion | bytes 6294528 | tf_op jit(solution)/shard_map/gather | solution.py:155
  20.8 0.0 copy-start.3
  20.8 0.0 copy-start.6
  20.8 1.2 constant_dynamic-slice_fusion
  22.0 27.3 %all_to_all.10 = bf16[8,1,96,512]{3,2,1,0:T(8,128)(2,1)} all-to-all(bf16[8,1,96,512]{3,2,1,0:T(8,128)(2,1)S(1)} %constant_dynamic-slice_fusion), channel_id=1, replica_groups=mesh['ep'=8,'tp'=4] {'ep'}, dimensions={0} | all-to-all | bytes 1572864 | tf_op jit(solution)/shard_map/all_to_all | solution.py:161
  49.4 0.0 all-gather.5.cloned.1.call-update
  49.4 0.0 all-gather.3.cloned.1.call-start
  49.4 0.0 copy-done.3
  49.5 0.1 fusion.55
  49.6 0.0 copy-done.6
  49.6 0.8 fusion.57
  50.4 0.0 all-gather.3.cloned.1.call-update
  50.5 0.0 reduce-scatter.2.cloned.1.call-start
  50.5 26.6 %all-gather.5.cloned.1.call-done = bf16[8,1,96,2048]{3,2,0,1:T(8,128)(2,1)} async-done(((bf16[8,1,96,512]{3,2,0,1:T(8,128)(2,1)}), bf16[8,1,96,2048]{3,2,0,1:T(8,128)(2,1)}) %all-gather.5.cloned.1.call-update) | async-done | bytes 3145744 | tf_op jit(solution)/shard_map/all_gather | solution.py:160
  77.1 8.3 %fusion.7 = f32[8,96,1024]{2,1,0:T(8,128)} fusion(bf16[1,2048,1024]{2,1,0:T(8,128)(2,1)} %param.24, bf16[8,1,96,2048]{3,2,0,1:T(8,128)(2,1)} %all-gather.5.cloned.1.call-done), kind=kOutput, calls=%fused_computation.11 | convolution fusion | flops 3221225472 | bytes 10485760 | tf_op jit(solution)/shard_map/sexd,edf->sexf/dot_general | solution.py:169
  85.4 12.9 %fusion.21 = bf16[8,1,96,2048]{3,2,0,1:T(8,128)(2,1)} fusion(bf16[1,1024,2048]{2,1,0:T(8,128)(2,1)} %param.25, f32[8,96,1024]{2,1,0:T(8,128)} %fusion.7, bf16[1,2048,1024]{2,1,0:T(8,128)(2,1)} %param.23, bf16[8,1,96,2048]{3,2,0,1:T(8,128)(2,1)} %all-gather.5.cloned.1.call-done), kind=kOutput, calls=%fused_computation.26 | convolution fusion | flops 6448742400 | bytes 17825792 | tf_op jit(solution)/shard_map/sexf,efd->sexd/dot_general | solution.py:173
  98.2 0.0 copy-start.5
  98.2 0.0 copy-start.4
  98.2 0.0 copy-start.7
  98.2 0.0 copy-start.8
  98.3 0.0 reduce-scatter.2.cloned.1.call-update
  98.3 0.7 copy-done.5
  99.0 0.2 copy-done.4
  99.2 0.1 copy.26
  99.3 0.0 copy-done.7
  99.3 0.1 copy.35
  99.5 0.1 multiply_cosine_fusion
  99.7 31.5 %all_gather.13 = bf16[2048,32]{0,1:T(8,128)(2,1)S(1)} all-gather(bf16[256,32]{0,1:T(8,128)(2,1)S(1)} %pad_maximum_fusion), channel_id=1, replica_groups=mesh['ep'=8,'tp'=4] {'ep'}, dimensions={0}, use_global_device_ids=true | all-gather | bytes 147456 | tf_op jit(solution)/shard_map/all_gather | solution.py:121
  131.2 0.0 all-gather.3.cloned.1.call-done
  131.3 0.0 copy-done.8
  131.3 2.9 %convolution_convert_fusion = bf16[2048,512]{0,1:T(8,128)(2,1)S(1)} fusion(bf16[2048,512]{1,0:T(8,128)(2,1)} %all-gather.3.cloned.1.call-done, bf16[512,512]{1,0:T(8,128)(2,1)S(1)} %copy-done.8), kind=kOutput, calls=%fused_computation.27 | convolution fusion | flops 1074790400 | bytes 4718592 | tf_op jit(solution)/shard_map/while/body/eval_jaxpr/dot_general | solution.py:115
  134.2 0.0 copy-start.2
  134.2 1.3 fusion.53
  135.5 0.1 copy-done.2
  135.6 5.0 %fusion.74 = (f32[256,4]{0,1:T(4,128)S(1)}, f32[256,4,2048]{0,2,1:T(8,128)}) fusion(bf16[2048,32]{0,1:T(8,128)(2,1)S(1)} %all_gather.13, bf16[256,4,16]{0,2,1:T(8,128)(2,1)S(1)} %get-tuple-element.21, bf16[256,4,16]{0,2,1:T(8,128)(2,1)S(1)} %get-tuple-element.20, f32[4,2048,256]{2,1,0:T(8,128)S(1)} %fusion.53), kind=kOutput, calls=%fused_computation.91 | convolution fusion | flops 140639232 | bytes 16977920 | tf_op jit(solution)/shard_map/while/body/eval_jaxpr/qhr,kr->qhk/dot_general | solution.py:94
  140.6 28.6 %reduce-scatter.2.cloned.1.call-done = bf16[8,1,96,512]{3,2,0,1:T(8,128)(2,1)} async-done(((bf16[8,1,96,2048]{3,2,0,1:T(8,128)(2,1)}), bf16[8,1,96,512]{3,2,0,1:T(8,128)(2,1)}) %reduce-scatter.2.cloned.1.call-update) | async-done | bytes 786448 | tf_op jit(solution)/shard_map/reduce_scatter | solution.py:176
  169.2 5.5 %all-to-all-start.1 = ((bf16[8,1,96,512]{3,2,1,0:T(8,128)(2,1)}), bf16[8,1,96,512]{3,2,1,0:T(8,128)(2,1)S(1)}, u32[]{:S(2)}, u32[]{:S(2)}) async-start(bf16[8,1,96,512]{3,2,1,0:T(8,128)(2,1)} %bitcast.122), calls=%async_computation.2 | async-start | bytes 1572864 | tf_op jit(solution)/shard_map/all_to_all | solution.py:179
  174.7 0.0 copy-start.1
  174.7 4.6 %fusion.1 = f32[256,4]{0,1:T(4,128)S(1)} fusion(f32[256,4,2048]{0,2,1:T(8,128)} %get-tuple-element.40, f32[256,4]{0,1:T(4,128)S(1)} %get-tuple-element.39), kind=kLoop, calls=%fused_computation.6 | loop fusion | flops 4193280 | bytes 8396800 | tf_op jit(solution)/shard_map/while/body/eval_jaxpr/reduce_sum | solution.py:99
  179.4 1.1 copy-done.1
  180.5 2.7 %fusion.41 = bf16[256,4,64]{0,2,1:T(8,128)(2,1)S(1)} fusion(f32[256,4,2048]{0,2,1:T(8,128)S(1)} %copy-done.1, f32[256,4]{0,1:T(4,128)S(1)} %get-tuple-element.39, bf16[2048,4,128]{0,2,1:T(8,128)(2,1)} %bitcast.119, f32[256,4]{0,1:T(4,128)S(1)} %get-tuple-element.25, f32[256,4]{0,1:T(4,128)S(1)} %get-tuple-element.24), kind=kOutput, calls=%fused_computation.38 | convolution fusion | flops 272826368 | bytes 9580544 | tf_op jit(solution)/shard_map/while/body/eval_jaxpr/qhk,khd->qhd/dot_general | solution.py:100
  183.1 6.5 %all_gather.14 = bf16[256,1024]{0,1:T(8,128)(2,1)S(1)} all-gather(bf16[256,256]{0,1:T(8,128)(2,1)S(1)} %bitcast.123), channel_id=1, replica_groups=mesh['ep'=8,'tp'=4] {'tp'}, dimensions={1}, use_global_device_ids=true | all-gather | bytes 655360 | tf_op jit(solution)/shard_map/all_gather | solution.py:140
  189.6 0.0 copy-done
  189.6 1.2 convolution_convert_fusion.1
  190.8 4.0 %all-to-all-done.1 = bf16[8,1,96,512]{3,2,1,0:T(8,128)(2,1)S(1)} async-done(((bf16[8,1,96,512]{3,2,1,0:T(8,128)(2,1)}), bf16[8,1,96,512]{3,2,1,0:T(8,128)(2,1)S(1)}, u32[]{:S(2)}, u32[]{:S(2)}) %all-to-all-start.1) | async-done | bytes 786464 | tf_op jit(solution)/shard_map/all_to_all | solution.py:179
  194.8 2.0 gather_fusion.1
  196.8 0.7 reshape.217
  197.4 2.1 multiply_reduce_fusion
  (17 shorter events, 0.2 us)
Async XLA Ops:
  7.2 182.5 %copy-start = (bf16[1024,512]{1,0:T(8,128)(2,1)S(1)}, bf16[1024,512]{1,0:T(8,128)(2,1)}, u32[]{:S(2)}) copy-start(bf16[1024,512]{1,0:T(8,128)(2,1)} %param.18) | copy-start | bytes 3145732
  7.2 69.9 %all-gather.5.cloned.1.call-start = ((), (), s32[]{:S(2)}) async-start(), calls=%async_computation.4 | async-start | bytes 3932160 | tf_op jit(solution)/shard_map/all_gather | solution.py:160
  20.8 28.6 %copy-start.3 = (bf16[256,512]{1,0:T(8,128)(2,1)S(1)}, bf16[256,512]{1,0:T(8,128)(2,1)}, u32[]{:S(2)}) copy-start(bf16[256,512]{1,0:T(8,128)(2,1)} %param.14) | copy-start | bytes 786436
  20.8 28.8 %copy-start.6 = (f32[512]{0:T(512)S(1)}, f32[512]{0:T(512)}, u32[]{:S(2)}) copy-start(f32[512]{0:T(512)} %param.16) | copy-start | bytes 6148
  49.4 81.8 %all-gather.3.cloned.1.call-start = ((), (), s32[]{:S(2)}) async-start(), calls=%async_computation.3 | async-start | bytes 2359296 | tf_op jit(solution)/shard_map/all_gather | solution.py:120
  50.5 118.7 %reduce-scatter.2.cloned.1.call-start = ((), (), s32[]{:S(2)}) async-start(), calls=%async_computation.5 | async-start | bytes 3932160 | tf_op jit(solution)/shard_map/reduce_scatter | solution.py:176
  98.2 0.7 copy-start.5
  98.2 0.9 copy-start.4
  98.2 1.1 copy-start.7
  98.2 33.0 %copy-start.8 = (bf16[512,512]{1,0:T(8,128)(2,1)S(1)}, bf16[512,512]{1,0:T(8,128)(2,1)}, u32[]{:S(2)}) copy-start(bf16[512,512]{1,0:T(8,128)(2,1)} %param.17) | copy-start | bytes 1572868
  134.2 1.4 copy-start.2
  169.2 25.6 %all-to-all-start.1 = ((bf16[8,1,96,512]{3,2,1,0:T(8,128)(2,1)}), bf16[8,1,96,512]{3,2,1,0:T(8,128)(2,1)S(1)}, u32[]{:S(2)}, u32[]{:S(2)}) async-start(bf16[8,1,96,512]{3,2,1,0:T(8,128)(2,1)} %bitcast.122), calls=%async_computation.2 | async-start | bytes 1572864 | tf_op jit(solution)/shard_map/all_to_all | solution.py:179
  174.7 5.8 %copy-start.1 = (f32[256,4,2048]{0,2,1:T(8,128)S(1)}, f32[256,4,2048]{0,2,1:T(8,128)}, u32[]{:S(2)}) copy-start(f32[256,4,2048]{0,2,1:T(8,128)} %get-tuple-element.40) | copy-start | bytes 25165828
Sparse Core Ops, SparseCore 0:
  49.5 27.5 all-gather.4
  79.8 50.4 all-gather.2
  132.8 36.3 reduce-scatter.1
where the time goes:
time: 206 us
  blocking collectives  65.3 us (32%)
  waiting for transfers between devices  59.3 us (29%)
  matrix products  34.2 us (17%)
  local copies, waits for them, and re-layouts  14.7 us (7%)
  between operations  14 us (7%)
  other arithmetic  12.9 us (6%)
  starting transfers between devices  5.61 us (3%)
    all_gather x1, blocking collectives, local(): piece_rope = lax.all_gather(key_rope, 'ep', axis=0, tiled=True)  31.5 us
    reduce_scatter x1, waiting for transfers between devices, local(): lax.psum_scatter(partial_out.astype(jnp.bfloat16), 'tp', scatter_dimensio...  28.6 us
    all_to_all x1, blocking collectives, local(): lax.all_to_all(own_columns, 'ep', split_axis=0, concat_axis=0, tiled=True)  27.3 us
    all_gather x1, waiting for transfers between devices, local(): lax.all_gather(lax.all_to_all(own_columns, 'ep', split_axis=0, concat_axi...  26.6 us
    dot_general x1, matrix products, local(): jnp.einsum('sexf,efd->sexd', hidden, down_weight, preferred_element_type=...  12.9 us
    dot_general x1, matrix products, local(): jnp.einsum('sexd,edf->sexf', arrived_whole, up_weight, preferred_element_...  8.26 us
    all_gather x1, blocking collectives, local(): lax.all_gather(attended, 'tp', axis=1, tiled=True)  6.5 us
    all_to_all x1, starting transfers between devices, local(): lax.all_to_all(summed, 'ep', split_axis=0, concat_axis=0, tiled=True)  5.49 us
  transfers between devices with their start and end apart: 4, of which 3 were waited for; matrix products, arithmetic and copies ran while one was open for 20% of the time, Pallas kernels for 0%

commit v1 on v0

v1 whole, which is shorter than its diff:
```python
import functools

import jax
import jax.numpy as jnp
from jax import lax
from jax.experimental import pallas as pl
from jax.experimental.pallas import tpu as pltpu
from jax.sharding import PartitionSpec as P

PLAIN_HEAD_DIM = 64
ROPE = 32
VALUE_HEAD_DIM = 64
LANES = 128
CORES = 2
RELAY_GROUPS = 4
CHUNKS = 2


EPSILON = 1e-06
ROPE_BASE_VALUE = 10000.0


def rms_scale(values, gain_vector):
    floats = values.astype(jnp.float32)
    return (
        floats
        * lax.rsqrt(jnp.mean(floats * floats, axis=-1, keepdims=True) + EPSILON)
        * gain_vector
    )


def rotary(values, positions):
    full_width = values.shape[-1]
    half_dim = full_width // 2
    frequency = ROPE_BASE_VALUE ** (-jnp.arange(half_dim, dtype=jnp.float32) * 2.0 / full_width)
    angles = positions[..., None] * frequency
    cosine = jnp.cos(angles)
    sine_part = jnp.sin(angles)
    first_half = values[..., :half_dim]
    second_half = values[..., half_dim:]
    return jnp.concatenate(
        [
            first_half * cosine - second_half * sine_part,
            second_half * cosine + first_half * sine_part,
        ],
        axis=-1,
    )


def merge_rows(block):
    return block.reshape(block.shape[0] * block.shape[1], block.shape[2])


def fused(
    n_ep,
    n_tp,
    heads,
    scale,
    q_ref,
    lat_ref,
    wkv_ref,
    wo_ref,
    moe_ref,
    wg_hbm,
    wu_hbm,
    wd_hbm,
    att_out,
    back,
    wg,
    wu,
    wd,
    g_lat,
    g_moe,
    g_att,
    kv,
    hidden,
    part,
    r1,
    s2,
    r2,
    tot,
    wsem,
    loc_sem,
    lat_a,
    lat_y,
    lat_c,
    moe_a,
    moe_y,
    moe_c,
    att_y,
    att_c,
    red_c,
    red_y,
    ret_a,
):
    me = lax.axis_index("ep")
    tp = lax.axis_index("tp")
    n_y = n_tp // CORES
    my_y = tp // CORES
    my_c = lax.rem(tp, CORES)
    mate = my_y * CORES + (1 - my_c)
    groups = min(RELAY_GROUPS, n_ep)
    per = n_ep // groups
    sends = []

    def to(src, dst, sems, index, ep_id, tp_id):
        copy = pltpu.make_async_remote_copy(
            src_ref=src,
            dst_ref=dst,
            send_sem=sems.at[(0,) + index],
            recv_sem=sems.at[(1,) + index],
            device_id=(ep_id, tp_id),
            device_id_type=pl.DeviceIdType.MESH,
        )
        copy.start()
        sends.append(copy)
        return copy

    barrier = pltpu.get_barrier_semaphore()
    for d in range(1, n_ep):
        pl.semaphore_signal(
            barrier,
            inc=1,
            device_id=(lax.rem(me + d, n_ep), tp),
            device_id_type=pl.DeviceIdType.MESH,
        )
    for d in range(1, n_tp):
        pl.semaphore_signal(
            barrier,
            inc=1,
            device_id=(me, lax.rem(tp + d, n_tp)),
            device_id_type=pl.DeviceIdType.MESH,
        )
    pl.semaphore_wait(barrier, n_ep + n_tp - 2)

    def scatter(kind, buffer, sems, source):
        copies = [pltpu.make_async_copy(source(me), buffer.at[tp, 0], loc_sem.at[kind])]
        copies[0].start()
        for d in range(1, n_ep):
            peer = lax.rem(me + d, n_ep)
            copies.append(to(source(peer), buffer.at[tp, d], sems, (d,), peer, tp))
        return copies

    lat_in = scatter(0, g_lat, lat_a, lambda peer: lat_ref)
    moe_in = scatter(1, g_moe, moe_a, lambda peer: moe_ref.at[peer])
    weights = []
    for i, (source, target) in enumerate(((wg_hbm, wg), (wu_hbm, wu), (wd_hbm, wd))):
        copy = pltpu.make_async_copy(source, target, wsem.at[i])
        copy.start()
        weights.append(copy)

    class Relay:
        def __init__(self, copies, buffer, ysem, csem):
            self.copies, self.buffer, self.ysem, self.csem = copies, buffer, ysem, csem
            self.y, self.c = {}, {}

        def view(self, t, g):
            return self.buffer.at[t, pl.ds(g * per, per)]

        def spread(self, g):
            for d in range(g * per, (g + 1) * per):
                if d == 0:
                    self.copies[0].wait()
                else:
                    self.copies[d].wait_recv()
            self.y[g] = []
            for o in range(1, n_y):
                other = lax.rem(my_y + o, n_y) * CORES + my_c
                self.y[g].append(
                    to(self.view(tp, g), self.view(tp, g), self.ysem, (o, g), me, other)
                )
            self.c[g] = [to(self.view(tp, g), self.view(tp, g), self.csem, (0, g), me, mate)]

        def forward(self, g):
            for o in range(1, n_y):
                self.y[g][o - 1].wait_recv()
                came = lax.rem(my_y + n_y - o, n_y) * CORES + my_c
                self.c[g].append(
                    to(self.view(came, g), self.view(came, g), self.csem, (o, g), me, mate)
                )

        def finish(self, g):
            for copy in self.c[g]:
                copy.wait_recv()

    lat = Relay(lat_in, g_lat, lat_y, lat_c)
    moe = Relay(moe_in, g_moe, moe_y, moe_c)
    for g in range(groups):
        lat.spread(g)
        if g > 0:
            lat.forward(g - 1)
    lat.forward(groups - 1)
    for g in range(groups):
        lat.finish(g)
    moe.spread(0)

    block = n_ep * lat_ref.shape[0]
    latent = wkv_ref.shape[0]

    def expand(t, carry):
        rows = merge_rows(g_lat[t])
        kv[pl.ds(pl.multiple_of(t * block, block), block), :] = jnp.dot(
            rows[:, :latent], wkv_ref[...], preferred_element_type=jnp.float32
        ).astype(jnp.bfloat16)
        return carry

    lax.fori_loop(0, n_tp, expand, 0)
    whole_lat = g_lat.reshape(n_tp * block, g_lat.shape[3])
    row_block = q_ref.shape[0]
    step = 0
    pending = [lambda g=g: moe.spread(g) for g in range(1, groups)]
    done_heads = []
    lane = lax.broadcasted_iota(jnp.int32, (1, LANES), 1)
    for h in range(heads):
        head = kv[:, h * LANES : (h + 1) * LANES]
        keys = jnp.where(lane < PLAIN_HEAD_DIM, head, whole_lat[:, latent : latent + LANES])
        scores = (
            lax.dot_general(
                q_ref[:, h * LANES : (h + 1) * LANES],
                keys,
                (((1,), (1,)), ((), ())),
                preferred_element_type=jnp.float32,
            )
            * scale
        )
        top = jnp.max(scores, axis=-1, keepdims=True)
        e = jnp.exp(scores - top)
        total = jnp.sum(e, axis=-1, keepdims=True)
        mixed = (
            jnp.dot(e.astype(jnp.bfloat16), head, preferred_element_type=jnp.float32) / total
        )
        if heads % 2 == 0:
            if h % 2 == 0:
                held = pltpu.roll(mixed, VALUE_HEAD_DIM, 1)
            else:
                g_att[tp, :, (h // 2) * LANES : (h // 2 + 1) * LANES] = jnp.where(
                    lane < VALUE_HEAD_DIM, held, mixed
                ).astype(jnp.bfloat16)
        else:
            g_att[tp, :, h * LANES : (h + 1) * LANES] = jnp.where(
                lane < PLAIN_HEAD_DIM, 0.0, mixed
            ).astype(jnp.bfloat16)
        if pending:
            pending.pop(0)()
            moe.forward(groups - len(pending) - 2)
    while pending:
        pending.pop(0)()
        moe.forward(groups - len(pending) - 2)
    moe.forward(groups - 1)

    own = g_att.at[tp]
    att_in = []
    for o in range(1, n_y):
        att_in.append(
            to(own, own, att_y, (o,), me, lax.rem(my_y + o, n_y) * CORES + my_c)
        )
    att_mate = [to(own, own, att_c, (0,), me, mate)]

    slots = n_ep // CHUNKS
    cap = moe_ref.shape[1]
    rows = slots * cap
    columns = moe_ref.shape[2]
    ff = wg.shape[1]
    tile = min(256, ff)

    def up(c):
        for g in range(groups):
            if (g * per) // slots == c:
                moe.finish(g)

        def one(f, carry):
            span = pl.ds(pl.multiple_of(f * tile, tile), tile)
            gate = jnp.zeros((rows, tile), jnp.float32)
            lift = jnp.zeros((rows, tile), jnp.float32)
            for t in range(n_tp):
                x = merge_rows(g_moe[t, c * slots : (c + 1) * slots])
                gate += jnp.dot(
                    x, wg[t * columns : (t + 1) * columns, span], preferred_element_type=jnp.float32
                )
                lift += jnp.dot(
                    x, wu[t * columns : (t + 1) * columns, span], preferred_element_type=jnp.float32
                )
            hidden[:, span] = (gate / (1.0 + jnp.exp(-gate)) * lift).astype(jnp.bfloat16)
            return carry

        lax.fori_loop(0, ff // tile, one, 0)

    def down(c):
        def one(t, carry):
            span = pl.ds(pl.multiple_of(t * columns, columns), columns)
            part[t, c * slots : (c + 1) * slots] = (
                jnp.dot(hidden[...], wd[:, span], preferred_element_type=jnp.float32)
                .astype(jnp.bfloat16)
                .reshape(slots, cap, columns)
            )
            return carry

        lax.fori_loop(0, n_tp, one, 0)

    reduce_c, reduce_y = {}, {}

    def swap(c):
        span = pl.ds(c * slots, slots)
        for o in list(range(1, n_y)) + [0]:
            y = lax.rem(my_y + o, n_y)
            reduce_c[c, o] = to(
                part.at[y * CORES + (1 - my_c), span], r1.at[o, span], red_c, (o, c), me, mate
            )

    def level_two(c):
        span = pl.ds(c * slots, slots)
        for o in range(1, n_y):
            y = lax.rem(my_y + o, n_y)
            reduce_c[c, o].wait_recv()
            s2[o, span] = (
                part[y * CORES + my_c, span].astype(jnp.float32) + r1[o, span].astype(jnp.float32)
            ).astype(jnp.bfloat16)
            reduce_y[c, o] = to(
                s2.at[o, span], r2.at[o, span], red_y, (o, c), me, y * CORES + my_c
            )

    returns = []

    def give_back(c):
        span = pl.ds(c * slots, slots)
        reduce_c[c, 0].wait_recv()
        total = part[tp, span].astype(jnp.float32) + r1[0, span].astype(jnp.float32)
        for o in range(1, n_y):
            reduce_y[c, o].wait_recv()
            total += r2[o, span].astype(jnp.float32)
        tot[span] = total.astype(jnp.bfloat16)
        for d in range(c * slots, (c + 1) * slots):
            if d == 0:
                back[0] = tot[0]
            else:
                peer = lax.rem(me + n_ep - d, n_ep)
                returns.append(to(tot.at[d], back.at[d], ret_a, (d,), peer, tp))

    def att_forward():
        for o in range(1, n_y):
            att_in[o - 1].wait_recv()
            came = g_att.at[lax.rem(my_y + n_y - o, n_y) * CORES + my_c]
            att_mate.append(to(came, came, att_c, (o,), me, mate))

    def project():
        for copy in att_mate:
            copy.wait_recv()
        width = g_att.shape[2]
        total = jnp.zeros(att_out.shape, jnp.float32)
        for t in range(n_tp):
            total += jnp.dot(
                g_att[t], wo_ref[t * width : (t + 1) * width, :], preferred_element_type=jnp.float32
            )
        att_out[...] = total.astype(jnp.bfloat16)

    for copy in weights:
        copy.wait()
    for c in range(CHUNKS):
        up(c)
        if c == 0:
            att_forward()
        if c > 0:
            level_two(c - 1)
        down(c)
        swap(c)
        if c > 0:
            give_back(c - 1)
    level_two(CHUNKS - 1)
    project()
    give_back(CHUNKS - 1)
    for copy in returns:
        copy.wait_recv()
    for copy in sends:
        copy.wait_send()


def local(
    queries,
    compressed_key_value,
    rope_key,
    latent_norm_gain,
    latent_to_key_value,
    out_proj,
    moe_input,
    moe_gain,
    routes,
    route_weight,
    gate_weight,
    up_weight,
    down_weight,
):
    n_ep = lax.axis_size("ep")
    n_tp = lax.axis_size("tp")
    me = lax.axis_index("ep")
    tp = lax.axis_index("tp")
    n_y = n_tp // CORES
    bf16 = jnp.bfloat16
    row_count = queries.shape[0]
    heads = latent_to_key_value.shape[1] // (PLAIN_HEAD_DIM + VALUE_HEAD_DIM)
    latent = compressed_key_value.shape[1]
    positions = (me * row_count + jnp.arange(row_count, dtype=jnp.int32)).astype(jnp.float32)
    q_heads = queries.reshape(row_count, heads, PLAIN_HEAD_DIM + ROPE)
    q_rope = rotary(q_heads[..., PLAIN_HEAD_DIM:].astype(jnp.float32), positions[:, None])
    pad = LANES - PLAIN_HEAD_DIM - ROPE
    q_all = jnp.concatenate(
        [
            q_heads[..., :PLAIN_HEAD_DIM],
            q_rope.astype(bf16),
            jnp.zeros((row_count, heads, pad), bf16),
        ],
        axis=-1,
    ).reshape(row_count, heads * LANES)
    share = row_count // n_tp
    cut = lambda x: lax.dynamic_slice_in_dim(x, tp * share, share, 0)
    lat = jnp.concatenate(
        [
            rms_scale(cut(compressed_key_value), latent_norm_gain).astype(bf16),
            jnp.zeros((share, PLAIN_HEAD_DIM), bf16),
            rotary(cut(rope_key).astype(jnp.float32), cut(positions)).astype(bf16),
            jnp.zeros((share, pad), bf16),
        ],
        axis=1,
    )
    if heads % 2 == 0:
        wo = out_proj
        att_width = heads * VALUE_HEAD_DIM
    else:
        wo = out_proj.reshape(n_tp * heads, VALUE_HEAD_DIM, out_proj.shape[1])
        wo = jnp.concatenate([jnp.zeros_like(wo), wo], axis=1)
        wo = wo.reshape(n_tp * heads * LANES, out_proj.shape[1])
        att_width = heads * LANES

    moe_rows, model_width = moe_input.shape
    top = routes.shape[1]
    capacity = 3 * moe_rows // n_ep
    places = -(-capacity // 16) * 16
    columns = model_width // n_tp
    flat = routes.reshape(-1)
    hot = (flat[:, None] == jnp.arange(n_ep, dtype=jnp.int32)[None, :]).astype(bf16)
    pairs = flat.shape[0]
    before = jnp.tril(jnp.ones((pairs, pairs), bf16), -1)
    earlier = jnp.dot(before, hot, preferred_element_type=jnp.float32)
    slot = jnp.sum(earlier * hot.astype(jnp.float32), axis=1).astype(jnp.int32)
    destination = (flat * places + slot).reshape(moe_rows, top)
    normed = rms_scale(moe_input, moe_gain).astype(bf16)
    own_normed = lax.dynamic_slice_in_dim(normed, tp * columns, columns, 1)
    place = jnp.arange(n_ep * places, dtype=jnp.int32)
    choose = jnp.zeros((n_ep * places, moe_rows), jnp.bool_)
    for k in range(top):
        choose = choose | (place[:, None] == destination[:, k][None, :])
    outgoing = jnp.dot(
        choose.astype(bf16), own_normed, preferred_element_type=jnp.float32
    ).astype(bf16)
    outgoing = outgoing.reshape(n_ep, places, columns)

    ff = gate_weight.shape[2]
    groups = min(RELAY_GROUPS, n_ep)
    vmem = pl.BlockSpec(memory_space=pltpu.VMEM)
    hbm = pl.BlockSpec(memory_space=pltpu.HBM)
    dma = lambda *shape: pltpu.SemaphoreType.DMA((2,) + shape)
    attention_out, back = pl.pallas_call(
        functools.partial(fused, n_ep, n_tp, heads, (PLAIN_HEAD_DIM + ROPE) ** (-0.5)),
        out_shape=(
            jax.ShapeDtypeStruct((row_count, out_proj.shape[1]), bf16),
            jax.ShapeDtypeStruct((n_ep, places, columns), bf16),
        ),
        in_specs=[vmem] * 5 + [hbm] * 3,
        out_specs=(vmem, vmem),
        scratch_shapes=[
            pltpu.VMEM((model_width, ff), bf16),
            pltpu.VMEM((model_width, ff), bf16),
            pltpu.VMEM((ff, model_width), bf16),
            pltpu.VMEM((n_tp, n_ep, share, latent + LANES), bf16),
            pltpu.VMEM((n_tp, n_ep, places, columns), bf16),
            pltpu.VMEM((n_tp, row_count, att_width), bf16),
            pltpu.VMEM((n_ep * row_count, heads * LANES), bf16),
            pltpu.VMEM((n_ep // CHUNKS * places, ff), bf16),
            pltpu.VMEM((n_tp, n_ep, places, columns), bf16),
            pltpu.VMEM((n_y, n_ep, places, columns), bf16),
            pltpu.VMEM((n_y, n_ep, places, columns), bf16),
            pltpu.VMEM((n_y, n_ep, places, columns), bf16),
            pltpu.VMEM((n_ep, places, columns), bf16),
            pltpu.SemaphoreType.DMA((3,)),
            pltpu.SemaphoreType.DMA((2,)),
            dma(n_ep),
            dma(n_y, groups),
            dma(n_y, groups),
            dma(n_ep),
            dma(n_y, groups),
            dma(n_y, groups),
            dma(n_y),
            dma(n_y),
            dma(n_y, CHUNKS),
            dma(n_y, CHUNKS),
            dma(n_ep),
        ],
        compiler_params=pltpu.CompilerParams(
            collective_id=0, has_side_effects=True, vmem_limit_bytes=60 * 1024 * 1024
        ),
        name="fused",
    )(
        q_all,
        lat,
        latent_to_key_value,
        wo,
        outgoing,
        gate_weight.reshape(model_width, ff),
        up_weight.reshape(model_width, ff),
        down_weight.reshape(ff, model_width),
    )
    flat_back = back.reshape(n_ep * places, columns)
    near = lax.rem(routes - me + n_ep, n_ep) * places + slot.reshape(moe_rows, top)
    expert_out = jnp.zeros((moe_rows, columns), jnp.float32)
    for k in range(top):
        pick = (near[:, k][:, None] == place[None, :]).astype(bf16)
        picked = jnp.dot(pick, flat_back, preferred_element_type=jnp.float32)
        expert_out = expert_out + picked * route_weight[:, k][:, None]
    return (attention_out, expert_out.astype(bf16))


def solution(mesh):
    return jax.shard_map(
        local,
        mesh=mesh,
        in_specs=(
            P("ep", "tp"),
            P("ep", None),
            P("ep", None),
            P(),
            P(None, "tp"),
            P(None, "tp"),
            P("ep", None),
            P(),
            P("ep", None),
            P("ep", None),
            P("ep", None, "tp"),
            P("ep", None, "tp"),
            P("ep", "tp", None),
        ),
        out_specs=(P("ep", "tp"), P("ep", "tp")),
        check_vma=False,
    )
```

time: 206 us -> 112 us (0.54)
  the two profiles are of different devices: /device:TPU:0 before, /device:TPU:20 now
where the time goes in v1:
time: 112 us
  Pallas kernels  97 us (87%)
  matrix products  5.54 us (5%)
  local copies, waits for them, and re-layouts  5.34 us (5%)
  other arithmetic  2.96 us (3%)
    pallas_call x1, Pallas kernels, local(): pl.pallas_call(functools.partial(fused, n_ep, n_tp, heads, (PLAIN_HEAD_DI...  97 us
    dot_general x2, matrix products, local(): picked = jnp.dot(pick, flat_back, preferred_element_type=jnp.float32)  3.83 us
    unnamed x16, local copies, waits for them, and re-layouts  2.37 us

profile of v1, /device:TPU:20, one launch (start us, length us, event | category | flops | bytes accessed | tf_op | source)
XLA Modules:
  0.0 111.8 jit_solution(16758659899799709909)
XLA Ops:
  0.6 0.0 copy-start
  0.6 0.0 copy-start.4
  0.7 0.0 copy-start.1
  0.7 0.1 dynamic_slice.14
  0.8 0.6 copy-done
  1.4 0.1 constant_dynamic-slice_fusion
  1.4 0.1 copy.50
  1.6 0.2 fusion.29
  1.8 1.0 fusion.19
  2.7 0.9 fusion.21
  3.7 0.7 concatenate.13.lat_ref
  4.4 0.8 dynamic-slice
  5.2 0.8 copy.46
  6.0 0.1 eq.76
  6.2 0.3 fusion.2
  6.5 0.1 convert_element_type.58
  6.7 0.1 copy.47
  6.8 0.0 copy-done.4
  6.8 0.0 copy-done.1
  6.8 0.0 copy-start.3
  6.8 0.2 convert_element_type.59
  7.1 0.3 multiply_reduce_fusion
  7.4 1.4 %convolution_convert_fusion = bf16[768,512]{1,0:T(8,128)(2,1)} fusion(s32[256]{0:T(256)S(1)} %bitcast.28, s32[256]{0:T(256)S(1)} %bitcast.29, f32[256,2048]{1,0:T(8,128)S(1)} %convert_element_type.59, s32[]{:T(128)S(6)} %select_n.14, f32[512]{0:T(512)S(1)} %dynamic-slice, f32[256]{0:T(256)S(1)} %add_rsqrt_fusion), kind=kOutput, calls=%fused_computation.1 | convolution fusion | flops 202702848 | bytes 1315844 | tf_op jit(solution)/shard_map/dot_general | solution.py:451
  8.7 0.1 multiply_cosine_fusion.1
  8.9 0.0 copy-done.3
  8.9 0.1 copy.42
  9.1 0.1 pad.3.clone
  9.2 0.1 maximum_maximum_fusion
  9.3 0.8 copy.49.q_ref
  10.1 0.0 copy-start.5
  10.1 97.0 %fused.1 = (bf16[256,512]{1,0:T(8,128)(2,1)}, bf16[8,96,512]{2,1,0:T(8,128)(2,1)}) custom-call(bf16[256,512]{1,0:T(8,128)(2,1)} %copy.49.q_ref, bf16[64,640]{1,0:T(8,128)(2,1)} %concatenate.13.lat_ref, bf16[512,512]{1,0:T(8,128)(2,1)} %wkv_ref.1, bf16[1024,512]{1,0:T(8,128)(2,1)} %wo_ref.1, bf16[8,96,512]{2,1,0:T(8,128)(2,1)} %bitcast.19, ...), custom_call_target="tpu_custom_call" | custom-call | tf_op jit(solution)/shard_map/fused/pallas_call | solution.py:461
  107.2 0.0 copy-start.2
  107.2 0.0 copy-done.5
  107.2 1.6 %convolution_multiply_fusion.1 = f32[256,512]{1,0:T(8,128)S(1)} fusion(bf16[768,512]{1,0:T(8,128)(2,1)} %bitcast.20, s32[256]{0:T(256)S(1)} %bitcast.27, f32[256]{0:T(256)S(1)} %bitcast.26), kind=kOutput, calls=%fused_computation.4 | convolution fusion | flops 201654272 | bytes 1312768 | tf_op jit(solution)/shard_map/dot_general | solution.py:516
  108.8 2.2 %fusion.1 = bf16[256,512]{1,0:T(8,128)(2,1)} fusion(f32[256,512]{1,0:T(8,128)S(1)} %convolution_multiply_fusion.1, bf16[768,512]{1,0:T(8,128)(2,1)} %bitcast.21, s32[256]{0:T(256)S(1)} %bitcast.25, f32[256]{0:T(256)S(1)} %bitcast.24), kind=kOutput, calls=%fused_computation.5 | convolution fusion | flops 201916416 | bytes 1574912 | tf_op jit(solution)/shard_map/dot_general | solution.py:516
  111.0 0.0 copy-done.2
  111.1 0.7 copy.52
  (16 shorter events, 0.1 us)
Async XLA Ops:
  0.6 0.7 copy-start
  0.6 6.1 %copy-start.4 = (s32[256,2]{0,1:T(2,128)S(1)}, s32[256,2]{0,1:T(2,128)}, u32[]{:S(2)}) copy-start(s32[256,2]{0,1:T(2,128)} %param.21) | copy-start | bytes 6148
  0.7 6.1 %copy-start.1 = (bf16[256,2048]{1,0:T(8,128)(2,1)S(1)}, bf16[256,2048]{1,0:T(8,128)(2,1)}, u32[]{:S(2)}) copy-start(bf16[256,2048]{1,0:T(8,128)(2,1)} %param.19) | copy-start | bytes 3145732
  6.8 2.1 %copy-start.3 = (bf16[256,384]{1,0:T(8,128)(2,1)S(1)}, bf16[256,384]{1,0:T(8,128)(2,1)}, u32[]{:S(2)}) copy-start(bf16[256,384]{1,0:T(8,128)(2,1)} %param.13) | copy-start | bytes 589828
  10.1 97.1 %copy-start.5 = (f32[256,2]{0,1:T(2,128)S(1)}, f32[256,2]{0,1:T(2,128)}, u32[]{:S(2)}) copy-start(f32[256,2]{0,1:T(2,128)} %param.22) | copy-start | bytes 6148
  107.2 3.9 %copy-start.2 = (bf16[256,512]{1,0:T(8,128)(2,1)S(1)}, bf16[256,512]{1,0:T(8,128)(2,1)}, u32[]{:S(2)}) copy-start(bf16[256,512]{1,0:T(8,128)(2,1)} %get-tuple-element.24) | copy-start | bytes 786436

commit v2 on v1

--- a/solution.py
+++ b/solution.py
@@ -45,6 +45,13 @@
         ],
         axis=-1,
     )
+
+
+def ep_shape(n_ep):
+    nx = 2 if n_ep % 2 == 0 else 1
+    nz = n_ep // nx
+    order = [0] if nz == 1 else [0, nz // 2] + [d for d in range(1, nz) if d != nz // 2]
+    return nx, nz, order
 
 
 def merge_rows(block):
@@ -82,7 +89,7 @@
     wsem,
     loc_sem,
     lat_a,
-    lat_y,
+    lat_x,
     lat_c,
     moe_a,
     moe_y,
@@ -101,7 +108,18 @@
     mate = my_y * CORES + (1 - my_c)
     groups = min(RELAY_GROUPS, n_ep)
     per = n_ep // groups
+    nx, nz, order = ep_shape(n_ep)
+    my_z = me // nx
+    my_x = lax.rem(me, nx)
     sends = []
+
+    def ahead(s):
+        z = lax.rem(my_z + order[s // nx], nz)
+        return z * nx + lax.rem(my_x + s % nx, nx)
+
+    def behind(s):
+        z = lax.rem(my_z + nz - order[s // nx], nz)
+        return z * nx + lax.rem(my_x + nx - s % nx, nx)
 
     def to(src, dst, sems, index, ep_id, tp_id):
         copy = pltpu.make_async_remote_copy(
@@ -133,16 +151,41 @@
         )
     pl.semaphore_wait(barrier, n_ep + n_tp - 2)
 
-    def scatter(kind, buffer, sems, source):
-        copies = [pltpu.make_async_copy(source(me), buffer.at[tp, 0], loc_sem.at[kind])]
-        copies[0].start()
-        for d in range(1, n_ep):
-            peer = lax.rem(me + d, n_ep)
-            copies.append(to(source(peer), buffer.at[tp, d], sems, (d,), peer, tp))
-        return copies
-
-    lat_in = scatter(0, g_lat, lat_a, lambda peer: lat_ref)
-    moe_in = scatter(1, g_moe, moe_a, lambda peer: moe_ref.at[peer])
+    moe_in = [pltpu.make_async_copy(moe_ref.at[me], g_moe.at[tp, 0], loc_sem.at[1])]
+    moe_in[0].start()
+    for s in range(1, n_ep):
+        moe_in.append(to(moe_ref.at[ahead(s)], g_moe.at[tp, s], moe_a, (s,), ahead(s), tp))
+    own_lat = my_c * nx
+    lat_in = [pltpu.make_async_copy(lat_ref, g_lat.at[own_lat, 0], loc_sem.at[0])]
+    lat_in[0].start()
+    for i in range(1, nz):
+        lat_in.append(
+            to(lat_ref, g_lat.at[own_lat, i], lat_a, (i,), ahead(i * nx), tp)
+        )
+    lat_over = []
+
+    def lat_relay(steps):
+        for i in steps:
+            if i == 0:
+                lat_in[0].wait()
+            else:
+                lat_in[i].wait_recv()
+            mine = g_lat.at[own_lat, i]
+            lat_over.append(to(mine, mine, lat_c, (0, i), me, mate))
+            if nx > 1:
+                side = g_lat.at[own_lat + 1, i]
+                lat_side.append(to(mine, side, lat_x, (i,), my_z * nx + 1 - my_x, tp))
+
+    lat_side = []
+
+    def lat_last():
+        for i, copy in enumerate(lat_side):
+            copy.wait_recv()
+            side = g_lat.at[own_lat + 1, i]
+            lat_over.append(to(side, side, lat_c, (1, i), me, mate))
+        for copy in lat_over:
+            copy.wait_recv()
+
     weights = []
     for i, (source, target) in enumerate(((wg_hbm, wg), (wu_hbm, wu), (wd_hbm, wd))):
         copy = pltpu.make_async_copy(source, target, wsem.at[i])
@@ -183,18 +226,8 @@
             for copy in self.c[g]:
                 copy.wait_recv()
 
-    lat = Relay(lat_in, g_lat, lat_y, lat_c)
     moe = Relay(moe_in, g_moe, moe_y, moe_c)
-    for g in range(groups):
-        lat.spread(g)
-        if g > 0:
-            lat.forward(g - 1)
-    lat.forward(groups - 1)
-    for g in range(groups):
-        lat.finish(g)
-    moe.spread(0)
-
-    block = n_ep * lat_ref.shape[0]
+    block = nz * lat_ref.shape[0]
     latent = wkv_ref.shape[0]
 
     def expand(t, carry):
@@ -204,57 +237,44 @@
         ).astype(jnp.bfloat16)
         return carry
 
-    lax.fori_loop(0, n_tp, expand, 0)
-    whole_lat = g_lat.reshape(n_tp * block, g_lat.shape[3])
-    row_block = q_ref.shape[0]
-    step = 0
-    pending = [lambda g=g: moe.spread(g) for g in range(1, groups)]
-    done_heads = []
+    whole_lat = g_lat.reshape(g_lat.shape[0] * block, g_lat.shape[3])
     lane = lax.broadcasted_iota(jnp.int32, (1, LANES), 1)
-    for h in range(heads):
-        head = kv[:, h * LANES : (h + 1) * LANES]
-        keys = jnp.where(lane < PLAIN_HEAD_DIM, head, whole_lat[:, latent : latent + LANES])
-        scores = (
-            lax.dot_general(
-                q_ref[:, h * LANES : (h + 1) * LANES],
-                keys,
-                (((1,), (1,)), ((), ())),
-                preferred_element_type=jnp.float32,
+    packed = 2 if heads % 2 == 0 else 1
+    att_in, att_mate = [], []
+
+    def attend(part_index):
+        for h in range(part_index * packed, (part_index + 1) * packed):
+            head = kv[:, h * LANES : (h + 1) * LANES]
+            keys = jnp.where(lane < PLAIN_HEAD_DIM, head, whole_lat[:, latent : latent + LANES])
+            scores = (
+                lax.dot_general(
+                    q_ref[:, h * LANES : (h + 1) * LANES],
+                    keys,
+                    (((1,), (1,)), ((), ())),
+                    preferred_element_type=jnp.float32,
+                )
+                * scale
             )
-            * scale
-        )
-        top = jnp.max(scores, axis=-1, keepdims=True)
-        e = jnp.exp(scores - top)
-        total = jnp.sum(e, axis=-1, keepdims=True)
-        mixed = (
-            jnp.dot(e.astype(jnp.bfloat16), head, preferred_element_type=jnp.float32) / total
-        )
-        if heads % 2 == 0:
-            if h % 2 == 0:
+            top = jnp.max(scores, axis=-1, keepdims=True)
+            e = jnp.exp(scores - top)
+            total = jnp.sum(e, axis=-1, keepdims=True)
+            mixed = (
+                jnp.dot(e.astype(jnp.bfloat16), head, preferred_element_type=jnp.float32) / total
+            )
+            if packed == 1:
+                mixed = jnp.where(lane < PLAIN_HEAD_DIM, 0.0, mixed)
+            elif h % 2 == 0:
                 held = pltpu.roll(mixed, VALUE_HEAD_DIM, 1)
             else:
-                g_att[tp, :, (h // 2) * LANES : (h // 2 + 1) * LANES] = jnp.where(
-                    lane < VALUE_HEAD_DIM, held, mixed
-                ).astype(jnp.bfloat16)
-        else:
-            g_att[tp, :, h * LANES : (h + 1) * LANES] = jnp.where(
-                lane < PLAIN_HEAD_DIM, 0.0, mixed
-            ).astype(jnp.bfloat16)
-        if pending:
-            pending.pop(0)()
-            moe.forward(groups - len(pending) - 2)
-    while pending:
-        pending.pop(0)()
-        moe.forward(groups - len(pending) - 2)
-    moe.forward(groups - 1)
-
-    own = g_att.at[tp]
-    att_in = []
-    for o in range(1, n_y):
-        att_in.append(
-            to(own, own, att_y, (o,), me, lax.rem(my_y + o, n_y) * CORES + my_c)
-        )
-    att_mate = [to(own, own, att_c, (0,), me, mate)]
+                mixed = jnp.where(lane < VALUE_HEAD_DIM, held, mixed)
+        g_att[tp, part_index] = mixed.astype(jnp.bfloat16)
+
+    def att_send(p):
+        own = g_att.at[tp, p]
+        for o in range(1, n_y):
+            other = lax.rem(my_y + o, n_y) * CORES + my_c
+            att_in.append((p, o, to(own, own, att_y, (o, p), me, other)))
+        att_mate.append(to(own, own, att_c, (0, p), me, mate))
 
     slots = n_ep // CHUNKS
     cap = moe_ref.shape[1]
@@ -333,41 +353,60 @@
             if d == 0:
                 back[0] = tot[0]
             else:
-                peer = lax.rem(me + n_ep - d, n_ep)
-                returns.append(to(tot.at[d], back.at[d], ret_a, (d,), peer, tp))
+                returns.append(to(tot.at[d], back.at[d], ret_a, (d,), behind(d), tp))
 
     def att_forward():
-        for o in range(1, n_y):
-            att_in[o - 1].wait_recv()
-            came = g_att.at[lax.rem(my_y + n_y - o, n_y) * CORES + my_c]
-            att_mate.append(to(came, came, att_c, (o,), me, mate))
+        for p, o, copy in att_in:
+            copy.wait_recv()
+            came = g_att.at[lax.rem(my_y + n_y - o, n_y) * CORES + my_c, p]
+            att_mate.append(to(came, came, att_c, (o, p), me, mate))
 
     def project():
         for copy in att_mate:
             copy.wait_recv()
-        width = g_att.shape[2]
         total = jnp.zeros(att_out.shape, jnp.float32)
         for t in range(n_tp):
+            x = jnp.concatenate([g_att[t, p] for p in range(g_att.shape[1])], axis=1)
+            width = x.shape[1]
             total += jnp.dot(
-                g_att[t], wo_ref[t * width : (t + 1) * width, :], preferred_element_type=jnp.float32
+                x, wo_ref[t * width : (t + 1) * width, :], preferred_element_type=jnp.float32
             )
         att_out[...] = total.astype(jnp.bfloat16)
 
+    parts = heads // packed
+    half = groups // 2
+    for g in range(half):
+        moe.spread(g)
+        if g > 0:
+            moe.forward(g - 1)
+    moe.forward(half - 1)
+    moe.spread(half)
     for copy in weights:
         copy.wait()
-    for c in range(CHUNKS):
-        up(c)
-        if c == 0:
-            att_forward()
-        if c > 0:
-            level_two(c - 1)
-        down(c)
-        swap(c)
-        if c > 0:
-            give_back(c - 1)
-    level_two(CHUNKS - 1)
+    up(0)
+    moe.forward(half)
+    for g in range(half + 1, groups):
+        moe.spread(g)
+        moe.forward(g)
+    down(0)
+    swap(0)
+    lat_relay(range(0, nz // 2))
+    up(1)
+    level_two(0)
+    down(1)
+    swap(1)
+    lat_relay(range(nz // 2, nz))
+    give_back(0)
+    level_two(1)
+    lat_last()
+    lax.fori_loop(0, g_lat.shape[0], expand, 0)
+    for p in range(parts):
+        attend(p)
+        if p == 0:
+            give_back(1)
+        att_send(p)
+    att_forward()
     project()
-    give_back(CHUNKS - 1)
     for copy in returns:
         copy.wait_recv()
     for copy in sends:
@@ -410,8 +449,9 @@
         ],
         axis=-1,
     ).reshape(row_count, heads * LANES)
-    share = row_count // n_tp
-    cut = lambda x: lax.dynamic_slice_in_dim(x, tp * share, share, 0)
+    share = row_count // CORES
+    nx, nz, order = ep_shape(n_ep)
+    cut = lambda x: lax.dynamic_slice_in_dim(x, lax.rem(tp, CORES) * share, share, 0)
     lat = jnp.concatenate(
         [
             rms_scale(cut(compressed_key_value), latent_norm_gain).astype(bf16),
@@ -423,12 +463,12 @@
     )
     if heads % 2 == 0:
         wo = out_proj
-        att_width = heads * VALUE_HEAD_DIM
+        parts = heads // 2
     else:
         wo = out_proj.reshape(n_tp * heads, VALUE_HEAD_DIM, out_proj.shape[1])
         wo = jnp.concatenate([jnp.zeros_like(wo), wo], axis=1)
         wo = wo.reshape(n_tp * heads * LANES, out_proj.shape[1])
-        att_width = heads * LANES
+        parts = heads
 
     moe_rows, model_width = moe_input.shape
     top = routes.shape[1]
@@ -470,9 +510,9 @@
             pltpu.VMEM((model_width, ff), bf16),
             pltpu.VMEM((model_width, ff), bf16),
             pltpu.VMEM((ff, model_width), bf16),
-            pltpu.VMEM((n_tp, n_ep, share, latent + LANES), bf16),
+            pltpu.VMEM((CORES * nx, nz, share, latent + LANES), bf16),
             pltpu.VMEM((n_tp, n_ep, places, columns), bf16),
-            pltpu.VMEM((n_tp, row_count, att_width), bf16),
+            pltpu.VMEM((n_tp, parts, row_count, LANES), bf16),
             pltpu.VMEM((n_ep * row_count, heads * LANES), bf16),
             pltpu.VMEM((n_ep // CHUNKS * places, ff), bf16),
             pltpu.VMEM((n_tp, n_ep, places, columns), bf16),
@@ -482,14 +522,14 @@
             pltpu.VMEM((n_ep, places, columns), bf16),
             pltpu.SemaphoreType.DMA((3,)),
             pltpu.SemaphoreType.DMA((2,)),
+            dma(nz),
+            dma(nz),
+            dma(nx, nz),
             dma(n_ep),
             dma(n_y, groups),
             dma(n_y, groups),
-            dma(n_ep),
-            dma(n_y, groups),
-            dma(n_y, groups),
-            dma(n_y),
-            dma(n_y),
+            dma(n_y, parts),
+            dma(n_y, parts),
             dma(n_y, CHUNKS),
             dma(n_y, CHUNKS),
             dma(n_ep),
@@ -509,7 +549,12 @@
         down_weight.reshape(ff, model_width),
     )
     flat_back = back.reshape(n_ep * places, columns)
-    near = lax.rem(routes - me + n_ep, n_ep) * places + slot.reshape(moe_rows, top)
+    far = lax.rem(routes // nx - me // nx + nz, nz)
+    step = jnp.zeros_like(far)
+    for i, dz in enumerate(order):
+        step = jnp.where(far == dz, i, step)
+    side = lax.rem(routes % nx - me % nx + nx, nx)
+    near = (step * nx + side) * places + slot.reshape(moe_rows, top)
     expert_out = jnp.zeros((moe_rows, columns), jnp.float32)
     for k in range(top):
         pick = (near[:, k][:, None] == place[None, :]).astype(bf16)

time: 112 us -> 94.3 us (0.84)
  the two profiles are of different devices: /device:TPU:20 before, /device:TPU:15 now
where the time goes in v2:
time: 94.3 us; the launch traced here: 94 us
  Pallas kernels  79.1 us (84%)
  matrix products  5.54 us (6%)
  local copies, waits for them, and re-layouts  5.4 us (6%)
  other arithmetic  3 us (3%)
    pallas_call x1, Pallas kernels, local(): pl.pallas_call(functools.partial(fused, n_ep, n_tp, heads, (PLAIN_HEAD_DI...  79.1 us
    dot_general x2, matrix products, local(): picked = jnp.dot(pick, flat_back, preferred_element_type=jnp.float32)  3.84 us
    unnamed x18, local copies, waits for them, and re-layouts  1.91 us

profile of v2, /device:TPU:15, one launch (start us, length us, event | category | flops | bytes accessed | tf_op | source)
XLA Modules:
  0.0 94.0 jit_solution(15665720205440601724)
XLA Ops:
  0.6 0.0 copy-start
  0.6 0.0 copy-start.1
  0.7 0.9 copy.47
  1.6 0.1 eq.92
  1.7 0.3 fusion.2
  2.1 0.1 convert_element_type.58
  2.2 0.7 broadcast_multiply_fusion
  2.9 0.1 copy.48
  3.1 0.7 broadcast_compare_fusion
  3.8 0.2 copy.54
  3.9 0.2 fusion.30
  4.2 0.3 slice_reduce_fusion
  4.5 0.8 dynamic-slice
  5.3 0.0 copy-done.1
  5.3 0.2 convert_element_type.59
  5.5 0.0 copy-start.2
  5.5 0.0 copy-start.5
  5.5 0.0 copy-start.4
  5.6 0.3 multiply_reduce_fusion
  5.9 1.4 %convolution_convert_fusion = bf16[768,512]{1,0:T(8,128)(2,1)} fusion(s32[256]{0:T(256)S(1)} %get-tuple-element.20, s32[256]{0:T(256)S(1)} %get-tuple-element.21, f32[256,2048]{1,0:T(8,128)S(1)} %convert_element_type.59, s32[]{:T(128)S(6)} %select_n.47, f32[512]{0:T(512)S(1)} %dynamic-slice, f32[256]{0:T(256)S(1)} %add_rsqrt_fusion), kind=kOutput, calls=%fused_computation.1 | convolution fusion | flops 202702848 | bytes 1315844 | tf_op jit(solution)/shard_map/dot_general | solution.py:491
  7.2 0.1 dynamic_slice.14
  7.3 0.0 copy-done
  7.3 0.1 copy.57
  7.4 0.3 fusion.39
  7.8 0.0 copy-done.2
  7.8 0.1 fusion.14
  7.9 0.0 copy-done.5
  7.9 0.1 fusion.16
  8.1 0.8 concatenate.13.lat_ref
  8.8 0.1 multiply_cosine_fusion.1
  9.0 0.0 copy-done.4
  9.0 0.1 copy.42
  9.2 0.1 pad.3.clone
  9.3 0.1 maximum_maximum_fusion
  9.4 0.8 copy.56.q_ref
  10.3 0.0 copy-start.6
  10.3 79.1 %fused.1 = (bf16[256,512]{1,0:T(8,128)(2,1)}, bf16[8,96,512]{2,1,0:T(8,128)(2,1)}) custom-call(bf16[256,512]{1,0:T(8,128)(2,1)} %copy.56.q_ref, bf16[128,640]{1,0:T(8,128)(2,1)} %concatenate.13.lat_ref, bf16[512,512]{1,0:T(8,128)(2,1)} %wkv_ref.1, bf16[1024,512]{1,0:T(8,128)(2,1)} %wo_ref.1, bf16[8,96,512]{2,1,0:T(8,128)(2,1)} %bitcast.19, ...), custom_call_target="tpu_custom_call" | custom-call | tf_op jit(solution)/shard_map/fused/pallas_call | solution.py:501
  89.4 0.0 copy-start.3
  89.4 0.0 copy-done.6
  89.4 1.6 %convolution_multiply_fusion.1 = f32[256,512]{1,0:T(8,128)S(1)} fusion(bf16[768,512]{1,0:T(8,128)(2,1)} %bitcast.15, s32[256]{0:T(256)S(1)} %get-tuple-element.7, f32[256]{0:T(256)S(1)} %bitcast.21), kind=kOutput, calls=%fused_computation.4 | convolution fusion | flops 201654272 | bytes 1312768 | tf_op jit(solution)/shard_map/dot_general | solution.py:561
  91.0 2.3 %fusion.1 = bf16[256,512]{1,0:T(8,128)(2,1)} fusion(f32[256,512]{1,0:T(8,128)S(1)} %convolution_multiply_fusion.1, bf16[768,512]{1,0:T(8,128)(2,1)} %bitcast.16, s32[256]{0:T(256)S(1)} %get-tuple-element.6, f32[256]{0:T(256)S(1)} %bitcast.20), kind=kOutput, calls=%fused_computation.5 | convolution fusion | flops 201916416 | bytes 1574912 | tf_op jit(solution)/shard_map/dot_general | solution.py:561
  93.3 0.0 copy-done.3
  93.3 0.7 copy.68
  (15 shorter events, 0.1 us)
Async XLA Ops:
  0.6 6.7 %copy-start = (bf16[256,32]{0,1:T(8,128)(2,1)S(1)}, bf16[256,32]{0,1:T(8,128)(2,1)}, u32[]{:S(2)}) copy-start(bf16[256,32]{0,1:T(8,128)(2,1)} %param.15) | copy-start | bytes 49156
  0.6 4.6 %copy-start.1 = (bf16[256,2048]{1,0:T(8,128)(2,1)S(1)}, bf16[256,2048]{1,0:T(8,128)(2,1)}, u32[]{:S(2)}) copy-start(bf16[256,2048]{1,0:T(8,128)(2,1)} %param.19) | copy-start | bytes 3145732
  5.5 2.3 %copy-start.2 = (bf16[256,512]{1,0:T(8,128)(2,1)S(1)}, bf16[256,512]{1,0:T(8,128)(2,1)}, u32[]{:S(2)}) copy-start(bf16[256,512]{1,0:T(8,128)(2,1)} %param.14) | copy-start | bytes 786436
  5.5 2.4 %copy-start.5 = (f32[512]{0:T(512)S(1)}, f32[512]{0:T(512)}, u32[]{:S(2)}) copy-start(f32[512]{0:T(512)} %param.16) | copy-start | bytes 6148
  5.5 3.4 %copy-start.4 = (bf16[256,384]{1,0:T(8,128)(2,1)S(1)}, bf16[256,384]{1,0:T(8,128)(2,1)}, u32[]{:S(2)}) copy-start(bf16[256,384]{1,0:T(8,128)(2,1)} %param.13) | copy-start | bytes 589828
  10.3 79.1 %copy-start.6 = (f32[256,2]{0,1:T(2,128)S(1)}, f32[256,2]{0,1:T(2,128)}, u32[]{:S(2)}) copy-start(f32[256,2]{0,1:T(2,128)} %param.22) | copy-start | bytes 6148
  89.4 3.9 %copy-start.3 = (bf16[256,512]{1,0:T(8,128)(2,1)S(1)}, bf16[256,512]{1,0:T(8,128)(2,1)}, u32[]{:S(2)}) copy-start(bf16[256,512]{1,0:T(8,128)(2,1)} %get-tuple-element.24) | copy-start | bytes 786436
